TPU v7x, 32 devices: a whole 2x2x4 slice. The times are simulated.
32 devices in a mesh: ra: 4 (over z), cb: 4 (over y, x), dp: 2 (over core).
Axes of the slice: x: 2, y: 2, z: 4, core: 2. Of those that a mesh axis runs over, the one named last changes fastest.
Arguments:
- tokens: bfloat16 [256, 2048], P('dp', 'ra'), may hold values from -200 to 200, as said below
- first_gain: float32 [2048], P('ra'), may hold values from 0.1 to 1.9
- first_gate: float32 [2048, 5632], P('ra', 'cb'), may hold values from -0.125 to 0.125
- first_gate_scale: float32 [5632], P('cb'), may hold values from 0.5 to 2
- first_up: float32 [2048, 5632], P('ra', 'cb'), may hold values from -0.125 to 0.125
- first_up_scale: float32 [5632], P('cb'), may hold values from 0.5 to 2
- first_down: float32 [5632, 2048], P('cb', 'ra'), may hold values from -0.078125 to 0.078125
- first_down_scale: float32 [2048], P('ra'), may hold values from 0.5 to 2
- second_gain: float32 [2048], P('ra'), may hold values from 0.1 to 1.9
- second_gate: float32 [2048, 5632], P('ra', 'cb'), may hold values from -0.125 to 0.125
- second_gate_scale: float32 [5632], P('cb'), may hold values from 0.5 to 2
- second_up: float32 [2048, 5632], P('ra', 'cb'), may hold values from -0.125 to 0.125
- second_up_scale: float32 [5632], P('cb'), may hold values from 0.5 to 2
- second_down: float32 [5632, 2048], P('cb', 'ra'), may hold values from -0.078125 to 0.078125
- second_down_scale: float32 [2048], P('ra'), may hold values from 0.5 to 2
Outputs:
- stream_out: bfloat16 [256, 2048], P('dp', 'ra')
Inputs may be any that keep to these rules, and one draw needn't show every extreme that they name: `tokens`: Per-token and per-feature magnitudes vary.
All inputs are finite; a program needn't handle non-finite values.
Results may differ from a plain program's by a relative error of at most 0.039.
Values may be sent and summed in bfloat16 or wider, within the bound.
A program may use at most 64 MiB of HBM per device.

v0:
```python
import jax
import jax.numpy as jnp
from jax import lax
from jax.sharding import PartitionSpec as P

D = 2048
EPS = 1e-06
RESID = 0.5


def sublayer(stream, gain, w_gate, gate_scale, w_up, up_scale, w_down, down_scale):
    values = stream.astype(jnp.float32)
    sum_sq = lax.psum(jnp.sum(values * values, -1), "ra")
    normed = (values * lax.rsqrt(sum_sq / D + EPS)[:, None] * gain).astype(jnp.bfloat16)
    part_gate = jnp.dot(normed, w_gate.astype(jnp.bfloat16), preferred_element_type=jnp.float32)
    part_up = jnp.dot(normed, w_up.astype(jnp.bfloat16), preferred_element_type=jnp.float32)
    gate, up = (
        lax.psum(part_gate.astype(jnp.bfloat16), "ra").astype(jnp.float32),
        lax.psum(part_up.astype(jnp.bfloat16), "ra").astype(jnp.float32),
    )
    hidden = (jax.nn.silu(gate * gate_scale) * (up * up_scale)).astype(jnp.bfloat16)
    partial_value = jnp.dot(hidden, w_down.astype(jnp.bfloat16), preferred_element_type=jnp.float32)
    branch = lax.psum(partial_value.astype(jnp.bfloat16), "cb").astype(jnp.float32)
    return (RESID * values + branch * down_scale).astype(jnp.bfloat16)


def body(
    tokens,
    first_gain,
    first_gate,
    first_gate_scale,
    first_up,
    first_up_scale,
    first_down,
    first_down_scale,
    second_gain,
    second_gate,
    second_gate_scale,
    second_up,
    second_up_scale,
    second_down,
    second_down_scale,
):
    middle = sublayer(
        tokens,
        first_gain,
        first_gate,
        first_gate_scale,
        first_up,
        first_up_scale,
        first_down,
        first_down_scale,
    )
    return sublayer(
        middle,
        second_gain,
        second_gate,
        second_gate_scale,
        second_up,
        second_up_scale,
        second_down,
        second_down_scale,
    )


def solution(mesh):
    in_specs = (
        P("dp", "ra"),
        P("ra"),
        P("ra", "cb"),
        P("cb"),
        P("ra", "cb"),
        P("cb"),
        P("cb", "ra"),
        P("ra"),
        P("ra"),
        P("ra", "cb"),
        P("cb"),
        P("ra", "cb"),
        P("cb"),
        P("cb", "ra"),
        P("ra"),
    )
    out_specs = P("dp", "ra")
    return jax.shard_map(body, mesh=mesh, in_specs=in_specs, out_specs=out_specs, check_vma=False)
```

profile of v0, /device:TPU:0, one launch (start us, length us, event | category | flops | bytes accessed | tf_op | source)
XLA Modules:
  0.0 218.9 jit_solution(4206691932930138170)
XLA Ops:
  6.5 0.0 copy-start.3
  6.5 0.0 copy-start.4
  6.5 0.0 copy-start
  6.5 0.0 all-reduce.13.cloned.1.call-start
  6.5 1.2 fusion.22
  7.7 13.5 %psum.56 = f32[128]{0:T(128)S(1)} all-reduce(f32[128]{0:T(128)S(1)} %fusion.22), channel_id=1, replica_groups=mesh['ra'=4,'cb'=4,'dp'=2] {'ra'}, use_global_device_ids=true, to_apply=%region_1.0 | all-reduce | flops 128 | bytes 1024 | tf_op jit(solution)/shard_map/psum | solution.py:13
  21.2 3.1 %convolution_convert_fusion.2 = bf16[128,1408]{1,0:T(8,128)(2,1)} fusion(f32[512,1408]{1,0:T(8,128)} %param.19, bf16[128,512]{1,0:T(8,128)(2,1)} %param.15, f32[512]{0:T(512)} %param.16, f32[128]{0:T(128)S(1)} %add_rsqrt_fusion.1), kind=kOutput, calls=%fused_computation.2 | convolution fusion | flops 185712640 | bytes 3377664 | tf_op jit(solution)/shard_map/dot_general | solution.py:16
  24.3 0.0 copy-done.3
  24.3 0.0 copy-done.4
  24.3 0.0 copy-done
  24.3 0.0 copy-start.9
  24.3 0.0 copy-start.10
  24.3 1.2 convolution_convert_fusion.3
  25.5 0.0 copy-start.6
  25.5 0.0 copy-start.1
  25.5 0.0 copy-start.5
  25.5 0.0 all-reduce.13.cloned.1.call-update
  25.5 0.0 all-reduce.7.cloned.1.call-start
  25.6 40.3 %all-reduce.13.cloned.1.call-done = (bf16[128,1408]{1,0:T(8,128)(2,1)}, bf16[128,1408]{1,0:T(8,128)(2,1)}) async-done(((bf16[128,1408]{1,0:T(8,128)(2,1)}, bf16[128,1408]{1,0:T(8,128)(2,1)}), (bf16[128,1408]{1,0:T(8,128)(2,1)}, bf16[128,1408]{1,0:T(8,128)(2,1)})) %all-reduce.13.cloned.1.call-update) | async-done | bytes 720912 | tf_op jit(solution)/shard_map/psum | solution.py:19
  65.9 0.0 copy-done.9
  65.9 0.0 copy-done.10
  65.9 3.2 %fusion.8 = bf16[128,512]{1,0:T(8,128)(2,1)} fusion(f32[1408,512]{1,0:T(8,128)} %param.21, bf16[128,1408]{1,0:T(8,128)(2,1)} %get-tuple-element.7, bf16[128,1408]{1,0:T(8,128)(2,1)} %get-tuple-element.8, f32[1408]{0:T(1024)S(1)} %copy-done.9, f32[1408]{0:T(1024)S(1)} %copy-done.10), kind=kOutput, calls=%fused_computation.12 | convolution fusion | flops 187138048 | bytes 3746816 | tf_op jit(solution)/shard_map/dot_general | solution.py:22
  69.1 0.0 all-reduce.7.cloned.1.call-update
  69.1 0.0 all-reduce.11.cloned.1.call-start
  69.1 41.8 %all-reduce.7.cloned.1.call-done = bf16[128,512]{1,0:T(8,128)(2,1)} async-done(((bf16[128,512]{1,0:T(8,128)(2,1)}), bf16[128,512]{1,0:T(8,128)(2,1)}) %all-reduce.7.cloned.1.call-update) | async-done | bytes 131088 | tf_op jit(solution)/shard_map/psum | solution.py:23
  111.0 0.0 copy-done.6
  111.0 1.0 fusion.27
  112.0 11.7 %psum.60 = f32[128]{0:T(128)S(1)} all-reduce(f32[128]{0:T(128)S(1)} %get-tuple-element.9), channel_id=1, replica_groups=mesh['ra'=4,'cb'=4,'dp'=2] {'ra'}, use_global_device_ids=true, to_apply=%region_6.7 | all-reduce | flops 128 | bytes 1024 | tf_op jit(solution)/shard_map/psum | solution.py:13
  123.7 0.0 copy-start.2
  123.7 0.0 copy-done.1
  123.7 0.0 copy-done.5
  123.7 1.2 convolution_convert_fusion
  124.9 0.8 copy-done.2
  125.7 0.0 copy-start.8
  125.7 0.0 copy-start.11
  125.7 0.0 copy-start.12
  125.7 1.2 convolution_convert_fusion.1
  126.8 0.0 all-reduce.11.cloned.1.call-update
  126.9 0.0 all-reduce.9.cloned.1.call-start
  126.9 39.3 %all-reduce.11.cloned.1.call-done = (bf16[128,1408]{1,0:T(8,128)(2,1)}, bf16[128,1408]{1,0:T(8,128)(2,1)}) async-done(((bf16[128,1408]{1,0:T(8,128)(2,1)}, bf16[128,1408]{1,0:T(8,128)(2,1)}), (bf16[128,1408]{1,0:T(8,128)(2,1)}, bf16[128,1408]{1,0:T(8,128)(2,1)})) %all-reduce.11.cloned.1.call-update) | async-done | bytes 720912 | tf_op jit(solution)/shard_map/psum | solution.py:19
  166.3 0.0 copy-done.8
  166.3 0.0 copy-done.11
  166.3 0.0 copy-done.12
  166.3 2.3 %fusion.11 = bf16[128,512]{1,0:T(8,128)(2,1)} fusion(f32[1408,512]{1,0:T(8,128)S(1)} %copy-done.8, bf16[128,1408]{1,0:T(8,128)(2,1)} %get-tuple-element.5, bf16[128,1408]{1,0:T(8,128)(2,1)} %get-tuple-element.6, f32[1408]{0:T(1024)S(1)} %copy-done.11, f32[1408]{0:T(1024)S(1)} %copy-done.12), kind=kOutput, calls=%fused_computation.13 | convolution fusion | flops 187138048 | bytes 3746816 | tf_op jit(solution)/shard_map/dot_general | solution.py:22
  168.5 0.0 all-reduce.9.cloned.1.call-update
  168.6 42.2 %all-reduce.9.cloned.1.call-done = bf16[128,512]{1,0:T(8,128)(2,1)} async-done(((bf16[128,512]{1,0:T(8,128)(2,1)}), bf16[128,512]{1,0:T(8,128)(2,1)}) %all-reduce.9.cloned.1.call-update) | async-done | bytes 131088 | tf_op jit(solution)/shard_map/psum | solution.py:23
  210.8 0.0 copy-done.7
  210.8 1.6 fusion.26
  (3 shorter events, 0.0 us)
Async XLA Ops:
  6.5 17.7 %copy-start.3 = (bf16[128,512]{1,0:T(8,128)(2,1)S(1)}, bf16[128,512]{1,0:T(8,128)(2,1)}, u32[]{:S(2)}) copy-start(bf16[128,512]{1,0:T(8,128)(2,1)} %param.15) | copy-start | bytes 393220
  6.5 17.7 %copy-start.4 = (f32[512]{0:T(512)S(1)}, f32[512]{0:T(512)}, u32[]{:S(2)}) copy-start(f32[512]{0:T(512)} %param.16) | copy-start | bytes 6148
  6.5 17.7 %copy-start = (f32[512,1408]{1,0:T(8,128)S(1)}, f32[512,1408]{1,0:T(8,128)}, u32[]{:S(2)}) copy-start(f32[512,1408]{1,0:T(8,128)} %param.17) | copy-start | bytes 8650756
  6.5 59.3 %all-reduce.13.cloned.1.call-start = ((), (), s32[]{:S(2)}) async-start(), calls=%async_computation.3 | async-start | bytes 1441792 | tf_op jit(solution)/shard_map/psum | solution.py:19
  24.3 41.6 %copy-start.9 = (f32[1408]{0:T(1024)S(1)}, f32[1408]{0:T(1024)}, u32[]{:S(2)}) copy-start(f32[1408]{0:T(1024)} %param.20) | copy-start | bytes 16900
  24.3 41.6 %copy-start.10 = (f32[1408]{0:T(1024)S(1)}, f32[1408]{0:T(1024)}, u32[]{:S(2)}) copy-start(f32[1408]{0:T(1024)} %param.18) | copy-start | bytes 16900
  25.5 85.5 %copy-start.6 = (f32[512]{0:T(512)S(1)}, f32[512]{0:T(512)}, u32[]{:S(2)}) copy-start(f32[512]{0:T(512)} %param.22) | copy-start | bytes 6148
  25.5 98.2 %copy-start.1 = (f32[512,1408]{1,0:T(8,128)S(1)}, f32[512,1408]{1,0:T(8,128)}, u32[]{:S(2)}) copy-start(f32[512,1408]{1,0:T(8,128)} %param.26) | copy-start | bytes 8650756
  25.5 98.2 %copy-start.5 = (f32[512]{0:T(512)S(1)}, f32[512]{0:T(512)}, u32[]{:S(2)}) copy-start(f32[512]{0:T(512)} %param.23) | copy-start | bytes 6148
  25.5 85.5 %all-reduce.7.cloned.1.call-start = ((), (), s32[]{:S(2)}) async-start(), calls=%async_computation | async-start | bytes 262144 | tf_op jit(solution)/shard_map/psum | solution.py:23
  69.1 97.2 %all-reduce.11.cloned.1.call-start = ((), (), s32[]{:S(2)}) async-start(), calls=%async_computation.2 | async-start | bytes 1441792 | tf_op jit(solution)/shard_map/psum | solution.py:19
  123.7 1.9 copy-start.2
  125.7 40.6 %copy-start.8 = (f32[1408,512]{1,0:T(8,128)S(1)}, f32[1408,512]{1,0:T(8,128)}, u32[]{:S(2)}) copy-start(f32[1408,512]{1,0:T(8,128)} %param.28) | copy-start | bytes 8650756
  125.7 40.6 %copy-start.11 = (f32[1408]{0:T(1024)S(1)}, f32[1408]{0:T(1024)}, u32[]{:S(2)}) copy-start(f32[1408]{0:T(1024)} %param.27) | copy-start | bytes 16900
  125.7 40.6 %copy-start.12 = (f32[1408]{0:T(1024)S(1)}, f32[1408]{0:T(1024)}, u32[]{:S(2)}) copy-start(f32[1408]{0:T(1024)} %param.25) | copy-start | bytes 16900
  126.8 83.9 %copy-start.7 = (f32[512]{0:T(512)S(1)}, f32[512]{0:T(512)}, u32[]{:S(2)}) copy-start(f32[512]{0:T(512)} %param.29) | copy-start | bytes 6148
  126.9 83.9 %all-reduce.9.cloned.1.call-start = ((), (), s32[]{:S(2)}) async-start(), calls=%async_computation.1 | async-start | bytes 262144 | tf_op jit(solution)/shard_map/psum | solution.py:23
Sparse Core Ops, SparseCore 0:
  25.6 40.1 all-reduce.12
  69.2 41.7 all-reduce.6
  127.0 39.2 all-reduce.10
  169.0 41.7 all-reduce.8
where the time goes:
time: 219 us
  waiting for transfers between devices  164 us (75%)
  blocking collectives  25.2 us (12%)
  between operations  13.2 us (6%)
  matrix products  12 us (5%)
  other arithmetic  3.83 us (2%)
    psum x2, waiting for transfers between devices, sublayer(): lax.psum(partial_value.astype(jnp.bfloat16), 'cb').astype(jnp.float32)  84 us
    psum x2, waiting for transfers between devices, sublayer(): lax.psum(part_up.astype(jnp.bfloat16), 'ra').astype(jnp.float32)  79.7 us
    psum x2, blocking collectives, sublayer(): sum_sq = lax.psum(jnp.sum(values * values, -1), 'ra')  25.2 us
    dot_general x2, matrix products, sublayer(): jnp.dot(hidden, w_down.astype(jnp.bfloat16), preferred_element_type=jnp.f...  5.45 us
  transfers between devices with their start and end apart: 4, of which 4 were waited for; matrix products, arithmetic and copies ran while one was open for 0% of the time, Pallas kernels for 0%

commit v1 on v0

--- a/solution.py
+++ b/solution.py
@@ -16,7 +16,7 @@
     part_up = jnp.dot(normed, w_up.astype(jnp.bfloat16), preferred_element_type=jnp.float32)
     gate, up = (
         lax.psum(part_gate.astype(jnp.bfloat16), "ra").astype(jnp.float32),
-        lax.psum(part_up.astype(jnp.bfloat16), "ra").astype(jnp.float32),
+        jnp.sum(lax.all_gather(part_up.astype(jnp.bfloat16), "ra"), axis=0).astype(jnp.float32),
     )
     hidden = (jax.nn.silu(gate * gate_scale) * (up * up_scale)).astype(jnp.bfloat16)
     partial_value = jnp.dot(hidden, w_down.astype(jnp.bfloat16), preferred_element_type=jnp.float32)

time: 219 us -> 278 us (1.27)
  waiting for transfers between devices: 164 us -> 218 us
  other arithmetic: 3.83 us -> 7.05 us
    all_gather x0 -> x2, waiting for transfers between devices: none -> 60.7 us  [sublayer(): lax.all_gather(part_up.astype(jnp.bfloat16), 'ra')]
    psum x2, waiting for transfers between devices: 79.7 us -> 72.3 us  [sublayer(): lax.psum(part_gate.astype(jnp.bfloat16), 'ra').astype(jnp.float32)]
    reduce_sum x0 -> x2, other arithmetic: none -> 3.21 us  [sublayer(): jnp.sum(lax.all_gather(part_up.astype(jnp.bfloat16), 'ra'), axis=0)]
  transfers between devices with their start and end apart: 4 -> 6, of which waited for: 4 -> 6; matrix products, arithmetic and copies ran while one was open for 0% -> 3% of each run, Pallas kernels for 0% -> 0%
where the time goes in v1:
time: 278 us
  waiting for transfers between devices  218 us (78%)
  blocking collectives  25.2 us (9%)
  matrix products  13.7 us (5%)
  between operations  13.5 us (5%)
  other arithmetic  7.05 us (3%)
    psum x2, waiting for transfers between devices, sublayer(): lax.psum(partial_value.astype(jnp.bfloat16), 'cb').astype(jnp.float32)  84.7 us
    psum x2, waiting for transfers between devices, sublayer(): lax.psum(part_gate.astype(jnp.bfloat16), 'ra').astype(jnp.float32)  72.3 us
    all_gather x2, waiting for transfers between devices, sublayer(): lax.all_gather(part_up.astype(jnp.bfloat16), 'ra')  60.7 us
    psum x2, blocking collectives, sublayer(): sum_sq = lax.psum(jnp.sum(values * values, -1), 'ra')  25.2 us
  transfers between devices with their start and end apart: 6, of which 6 were waited for; matrix products, arithmetic and copies ran while one was open for 3% of the time, Pallas kernels for 0%

profile of v1, /device:TPU:0, one launch (start us, length us, event | category | flops | bytes accessed | tf_op | source)
XLA Modules:
  0.0 277.6 jit_solution(10535501963997082981)
XLA Ops:
  6.5 0.0 copy-start.2
  6.5 0.0 copy-start.3
  6.5 0.0 all-gather.5.cloned.1.call-start
  6.5 1.2 fusion.22
  7.7 13.5 %psum.42 = f32[128]{0:T(128)S(1)} all-reduce(f32[128]{0:T(128)S(1)} %fusion.22), channel_id=1, replica_groups=mesh['ra'=4,'cb'=4,'dp'=2] {'ra'}, use_global_device_ids=true, to_apply=%region_1.0 | all-reduce | flops 128 | bytes 1024 | tf_op jit(solution)/shard_map/psum | solution.py:13
  21.2 3.1 %convolution_convert_fusion.2 = bf16[128,1408]{1,0:T(8,128)(2,1)} fusion(f32[512,1408]{1,0:T(8,128)} %param.19, bf16[128,512]{1,0:T(8,128)(2,1)} %param.15, f32[512]{0:T(512)} %param.16, f32[128]{0:T(128)S(1)} %add_rsqrt_fusion.1), kind=kOutput, calls=%fused_computation.2 | convolution fusion | flops 185712640 | bytes 3377664 | tf_op jit(solution)/shard_map/dot_general | solution.py:16
  24.3 0.0 copy-start.8
  24.3 0.0 all-gather.5.cloned.1.call-update
  24.3 0.0 all-reduce.5.cloned.1.call-start
  24.3 0.0 copy-done.2
  24.4 0.0 copy-done.3
  24.4 0.0 copy-done
  24.4 1.2 convolution_convert_fusion.3
  25.5 0.0 all-reduce.5.cloned.1.call-update
  25.6 0.0 all-reduce.7.cloned.1.call-start
  25.6 31.8 %all-gather.5.cloned.1.call-done = bf16[512,1408]{1,0:T(8,128)(2,1)} async-done(((bf16[128,1408]{1,0:T(8,128)(2,1)}), bf16[512,1408]{1,0:T(8,128)(2,1)}) %all-gather.5.cloned.1.call-update) | async-done | bytes 1441808 | tf_op jit(solution)/shard_map/all_gather | solution.py:19
  57.4 1.6 reduce_sum.43
  59.0 0.0 copy-start.1
  59.1 0.0 copy-start.4
  59.1 36.2 %all-reduce.5.cloned.1.call-done = bf16[128,1408]{1,0:T(8,128)(2,1)} async-done(((bf16[128,1408]{1,0:T(8,128)(2,1)}), bf16[128,1408]{1,0:T(8,128)(2,1)}) %all-reduce.5.cloned.1.call-update) | async-done | bytes 360464 | tf_op jit(solution)/shard_map/psum | solution.py:18
  95.3 0.0 copy-done.8
  95.3 0.0 copy-done.9
  95.3 3.1 %fusion.8 = bf16[128,512]{1,0:T(8,128)(2,1)} fusion(f32[1408,512]{1,0:T(8,128)} %param.21, bf16[128,1408]{1,0:T(8,128)(2,1)S(1)} %reduce_sum.43, bf16[128,1408]{1,0:T(8,128)(2,1)} %all-reduce.5.cloned.1.call-done, f32[1408]{0:T(1024)S(1)} %copy-done.8, f32[1408]{0:T(1024)S(1)} %copy-done.9), kind=kOutput, calls=%fused_computation.12 | convolution fusion | flops 187138048 | bytes 3746816 | tf_op jit(solution)/shard_map/dot_general | solution.py:22
  98.4 0.0 all-reduce.7.cloned.1.call-update
  98.4 0.0 all-gather.7.cloned.1.call-start
  98.5 42.1 %all-reduce.7.cloned.1.call-done = bf16[128,512]{1,0:T(8,128)(2,1)} async-done(((bf16[128,512]{1,0:T(8,128)(2,1)}), bf16[128,512]{1,0:T(8,128)(2,1)}) %all-reduce.7.cloned.1.call-update) | async-done | bytes 131088 | tf_op jit(solution)/shard_map/psum | solution.py:23
  140.6 0.0 copy-done.5
  140.6 1.0 fusion.27
  141.6 11.7 %psum.45 = f32[128]{0:T(128)S(1)} all-reduce(f32[128]{0:T(128)S(1)} %get-tuple-element.5), channel_id=1, replica_groups=mesh['ra'=4,'cb'=4,'dp'=2] {'ra'}, use_global_device_ids=true, to_apply=%region_6.7 | all-reduce | flops 128 | bytes 1024 | tf_op jit(solution)/shard_map/psum | solution.py:13
  153.3 0.0 copy-done.1
  153.3 0.0 copy-done.4
  153.3 1.2 convolution_convert_fusion
  154.5 0.0 all-gather.7.cloned.1.call-update
  154.5 0.0 all-reduce.9.cloned.1.call-start
  154.6 3.1 %convolution_convert_fusion.1 = bf16[128,1408]{1,0:T(8,128)(2,1)} fusion(f32[512,1408]{1,0:T(8,128)} %param.24, bf16[128,512]{1,0:T(8,128)(2,1)S(1)} %get-tuple-element.6, f32[512]{0:T(512)S(1)} %copy-done.4, f32[128]{0:T(128)S(1)} %add_rsqrt_fusion), kind=kOutput, calls=%fused_computation.1 | convolution fusion | flops 185712640 | bytes 3377664 | tf_op jit(solution)/shard_map/dot_general | solution.py:15
  157.7 0.0 all-reduce.9.cloned.1.call-update
  157.7 0.0 all-reduce.11.cloned.1.call-start
  157.8 28.9 %all-gather.7.cloned.1.call-done = bf16[512,1408]{1,0:T(8,128)(2,1)} async-done(((bf16[128,1408]{1,0:T(8,128)(2,1)}), bf16[512,1408]{1,0:T(8,128)(2,1)}) %all-gather.7.cloned.1.call-update) | async-done | bytes 1441808 | tf_op jit(solution)/shard_map/all_gather | solution.py:19
  186.7 1.6 reduce_sum.45
  188.3 36.1 %all-reduce.9.cloned.1.call-done = bf16[128,1408]{1,0:T(8,128)(2,1)} async-done(((bf16[128,1408]{1,0:T(8,128)(2,1)}), bf16[128,1408]{1,0:T(8,128)(2,1)}) %all-reduce.9.cloned.1.call-update) | async-done | bytes 360464 | tf_op jit(solution)/shard_map/psum | solution.py:18
  224.4 0.0 copy-done.7
  224.4 0.0 copy-done.10
  224.4 0.0 copy-done.11
  224.4 2.1 fusion.11
  226.5 0.0 all-reduce.11.cloned.1.call-update
  226.6 42.6 %all-reduce.11.cloned.1.call-done = bf16[128,512]{1,0:T(8,128)(2,1)} async-done(((bf16[128,512]{1,0:T(8,128)(2,1)}), bf16[128,512]{1,0:T(8,128)(2,1)}) %all-reduce.11.cloned.1.call-update) | async-done | bytes 131088 | tf_op jit(solution)/shard_map/psum | solution.py:23
  269.2 0.0 copy-done.6
  269.2 1.6 fusion.26
  (9 shorter events, 0.0 us)
Async XLA Ops:
  6.5 17.8 %copy-start.2 = (bf16[128,512]{1,0:T(8,128)(2,1)S(1)}, bf16[128,512]{1,0:T(8,128)(2,1)}, u32[]{:S(2)}) copy-start(bf16[128,512]{1,0:T(8,128)(2,1)} %param.15) | copy-start | bytes 393220
  6.5 17.8 %copy-start.3 = (f32[512]{0:T(512)S(1)}, f32[512]{0:T(512)}, u32[]{:S(2)}) copy-start(f32[512]{0:T(512)} %param.16) | copy-start | bytes 6148
  6.5 17.8 %copy-start = (f32[512,1408]{1,0:T(8,128)S(1)}, f32[512,1408]{1,0:T(8,128)}, u32[]{:S(2)}) copy-start(f32[512,1408]{1,0:T(8,128)} %param.17) | copy-start | bytes 8650756
  6.5 50.9 %all-gather.5.cloned.1.call-start = ((), (), s32[]{:S(2)}) async-start(), calls=%async_computation.4 | async-start | bytes 1802240 | tf_op jit(solution)/shard_map/all_gather | solution.py:19
  24.3 71.0 %copy-start.8 = (f32[1408]{0:T(1024)S(1)}, f32[1408]{0:T(1024)}, u32[]{:S(2)}) copy-start(f32[1408]{0:T(1024)} %param.20) | copy-start | bytes 16900
  24.3 71.0 %copy-start.9 = (f32[1408]{0:T(1024)S(1)}, f32[1408]{0:T(1024)}, u32[]{:S(2)}) copy-start(f32[1408]{0:T(1024)} %param.18) | copy-start | bytes 16900
  24.3 71.0 %all-reduce.5.cloned.1.call-start = ((), (), s32[]{:S(2)}) async-start(), calls=%async_computation | async-start | bytes 720896 | tf_op jit(solution)/shard_map/psum | solution.py:18
  25.6 115.0 %all-reduce.7.cloned.1.call-start = ((), (), s32[]{:S(2)}) async-start(), calls=%async_computation.1 | async-start | bytes 262144 | tf_op jit(solution)/shard_map/psum | solution.py:23
  57.4 83.2 %copy-start.5 = (f32[512]{0:T(512)S(1)}, f32[512]{0:T(512)}, u32[]{:S(2)}) copy-start(f32[512]{0:T(512)} %param.22) | copy-start | bytes 6148
  59.0 94.3 %copy-start.1 = (f32[512,1408]{1,0:T(8,128)S(1)}, f32[512,1408]{1,0:T(8,128)}, u32[]{:S(2)}) copy-start(f32[512,1408]{1,0:T(8,128)} %param.26) | copy-start | bytes 8650756
  59.1 94.3 %copy-start.4 = (f32[512]{0:T(512)S(1)}, f32[512]{0:T(512)}, u32[]{:S(2)}) copy-start(f32[512]{0:T(512)} %param.23) | copy-start | bytes 6148
  98.4 88.3 %all-gather.7.cloned.1.call-start = ((), (), s32[]{:S(2)}) async-start(), calls=%async_computation.5 | async-start | bytes 1802240 | tf_op jit(solution)/shard_map/all_gather | solution.py:19
  154.5 69.9 %copy-start.7 = (f32[1408,512]{1,0:T(8,128)S(1)}, f32[1408,512]{1,0:T(8,128)}, u32[]{:S(2)}) copy-start(f32[1408,512]{1,0:T(8,128)} %param.28) | copy-start | bytes 8650756
  154.5 69.9 %copy-start.10 = (f32[1408]{0:T(1024)S(1)}, f32[1408]{0:T(1024)}, u32[]{:S(2)}) copy-start(f32[1408]{0:T(1024)} %param.27) | copy-start | bytes 16900
  154.5 69.9 %copy-start.11 = (f32[1408]{0:T(1024)S(1)}, f32[1408]{0:T(1024)}, u32[]{:S(2)}) copy-start(f32[1408]{0:T(1024)} %param.25) | copy-start | bytes 16900
  154.5 69.9 %all-reduce.9.cloned.1.call-start = ((), (), s32[]{:S(2)}) async-start(), calls=%async_computation.2 | async-start | bytes 720896 | tf_op jit(solution)/shard_map/psum | solution.py:18
  157.7 111.5 %all-reduce.11.cloned.1.call-start = ((), (), s32[]{:S(2)}) async-start(), calls=%async_computation.3 | async-start | bytes 262144 | tf_op jit(solution)/shard_map/psum | solution.py:23
  186.7 82.5 %copy-start.6 = (f32[512]{0:T(512)S(1)}, f32[512]{0:T(512)}, u32[]{:S(2)}) copy-start(f32[512]{0:T(512)} %param.29) | copy-start | bytes 6148
Sparse Core Ops, SparseCore 0:
  24.4 32.9 all-gather.4
  59.8 35.4 all-reduce.4
  98.6 41.9 all-reduce.6
  154.7 31.9 all-gather.6
  188.9 35.4 all-reduce.8
  227.2 41.9 all-reduce.10
